TPU v7x, 32 devices: a whole 2x2x4 slice. The times are simulated.
32 devices in a mesh: fs: 8 (over z, y), tp: 4 (over x, core).
Axes of the slice: x: 2, y: 2, z: 4, core: 2. Of those that a mesh axis runs over, the one named last changes fastest.
Arguments:
- saved_input: bfloat16 [6144, 2048], P('fs'), may hold values from -6 to 6
- cot_inproj: bfloat16 [6144, 1024], P('fs', 'tp'), may hold values from -0.076171875 to 0.076171875
- cot_outproj: bfloat16 [6144, 1024], P('fs', 'tp'), may hold values from -0.076171875 to 0.076171875
- factor_inproj: bfloat16 [2048, 256], P('fs')
- factor_outproj: bfloat16 [2048, 256], P('fs')
- weight_inproj: float32 [2048, 1024], P('fs', 'tp'), may hold values from -0.125 to 0.125
- weight_outproj: float32 [2048, 1024], P('fs', 'tp'), may hold values from -0.125 to 0.125
- first_inproj: float32 [256, 1024], P('fs', 'tp'), may hold values from -6 to 6
- first_outproj: float32 [256, 1024], P('fs', 'tp'), may hold values from -6 to 6
- second_inproj: float32 [256, 1024], P('fs', 'tp'), may hold values from 0.25 to 4
- second_outproj: float32 [256, 1024], P('fs', 'tp'), may hold values from 0.25 to 4
Outputs:
- update_inproj: float32 [2048, 1024], P('fs', 'tp')
- update_outproj: float32 [2048, 1024], P('fs', 'tp')
- new_inproj: float32 [2048, 1024], P('fs', 'tp')
- new_outproj: float32 [2048, 1024], P('fs', 'tp')
- copy_inproj: bfloat16 [2048, 1024], P(None, 'tp')
- copy_outproj: bfloat16 [2048, 1024], P(None, 'tp')
- first_inproj_new: float32 [256, 1024], P('fs', 'tp')
- first_outproj_new: float32 [256, 1024], P('fs', 'tp')
- second_inproj_new: float32 [256, 1024], P('fs', 'tp')
- second_outproj_new: float32 [256, 1024], P('fs', 'tp')
All inputs are finite; a program needn't handle non-finite values.
Results may differ from a plain program's by a relative error of at most 0.00045.
Values may be sent and summed in bfloat16 or wider, within the bound.
No kernel may reach another device: no remote copies, remote signals or barrier semaphores. Data moves between devices by JAX's collectives and lax.ppermute only.
A program may use at most 64 MiB of HBM per device.

v0:
```python
import jax
import jax.numpy as jnp
from jax import lax
from jax.sharding import PartitionSpec as P


def contract_rows(left, right, precision):
    return lax.dot_general(
        left,
        right,
        (((0,), (0,)), ((), ())),
        precision=precision,
        preferred_element_type=jnp.float32,
    )


def on_device(
    saved_input,
    cot_inproj,
    cot_outproj,
    factor_inproj,
    factor_outproj,
    weight_inproj,
    weight_outproj,
    first_inproj,
    first_outproj,
    second_inproj,
    second_outproj,
):
    highest = lax.Precision.HIGHEST
    pieces = (
        lax.all_gather(factor_inproj, "fs", axis=0, tiled=True),
        lax.all_gather(factor_outproj, "fs", axis=0, tiled=True),
    )
    mapped_in = jnp.dot(saved_input, pieces[0], preferred_element_type=jnp.float32)
    mapped_out = jnp.dot(saved_input, pieces[1], preferred_element_type=jnp.float32)
    term_in = contract_rows(mapped_in, cot_inproj.astype(jnp.float32), highest)
    term_out = contract_rows(mapped_out, cot_outproj.astype(jnp.float32), highest)
    projected_in, projected_out = (
        lax.psum_scatter(term_in, "fs", scatter_dimension=0, tiled=True),
        lax.psum_scatter(term_out, "fs", scatter_dimension=0, tiled=True),
    )
    first_in_new = 0.8 * first_inproj + 0.2 * projected_in
    first_out_new = 0.8 * first_outproj + 0.2 * projected_out
    second_in_new = 0.9 * second_inproj + 0.1 * projected_in * projected_in
    second_out_new = 0.9 * second_outproj + 0.1 * projected_out * projected_out
    small_in = first_in_new / (jnp.sqrt(second_in_new) + 1e-08)
    small_out = first_out_new / (jnp.sqrt(second_out_new) + 1e-08)
    wide_in = factor_inproj.astype(jnp.float32)
    wide_out = factor_outproj.astype(jnp.float32)
    pieces = (
        lax.all_gather(small_in, "fs", axis=0, tiled=True),
        lax.all_gather(small_out, "fs", axis=0, tiled=True),
    )
    full_in = jnp.dot(wide_in, pieces[0], precision=highest)
    full_out = jnp.dot(wide_out, pieces[1], precision=highest)
    square_in, square_out = lax.psum(
        (jnp.sum(full_in * full_in), jnp.sum(full_out * full_out)), ("fs", "tp")
    )
    entries = float(full_in.shape[0] * full_in.shape[1] * lax.axis_size("fs") * lax.axis_size("tp"))
    update_in = full_in / jnp.sqrt(square_in / entries + 1e-06)
    update_out = full_out / jnp.sqrt(square_out / entries + 1e-06)
    fresh_in = weight_inproj - 0.02 * update_in
    fresh_out = weight_outproj - 0.02 * update_out
    copy_in, copy_out = (
        lax.all_gather(fresh_in.astype(jnp.bfloat16), "fs", axis=0, tiled=True),
        lax.all_gather(fresh_out.astype(jnp.bfloat16), "fs", axis=0, tiled=True),
    )
    return (
        update_in,
        update_out,
        fresh_in,
        fresh_out,
        copy_in,
        copy_out,
        first_in_new,
        first_out_new,
        second_in_new,
        second_out_new,
    )


def solution(mesh):
    return jax.shard_map(
        on_device,
        mesh=mesh,
        in_specs=(
            P("fs", None),
            P("fs", "tp"),
            P("fs", "tp"),
            P("fs", None),
            P("fs", None),
            P("fs", "tp"),
            P("fs", "tp"),
            P("fs", "tp"),
            P("fs", "tp"),
            P("fs", "tp"),
            P("fs", "tp"),
        ),
        out_specs=(
            P("fs", "tp"),
            P("fs", "tp"),
            P("fs", "tp"),
            P("fs", "tp"),
            P(None, "tp"),
            P(None, "tp"),
            P("fs", "tp"),
            P("fs", "tp"),
            P("fs", "tp"),
            P("fs", "tp"),
        ),
        check_vma=False,
    )
```

profile of v0, /device:TPU:0, one launch (start us, length us, event | category | flops | bytes accessed | tf_op | source)
XLA Modules:
  0.0 389.0 jit_solution(17355608462318028329)
XLA Ops:
  7.2 0.0 copy-start
  7.2 0.0 all-gather.5.cloned.1.call-start
  7.2 0.7 all-gather.5.cloned.1.call-update
  7.9 0.0 all-gather.7.cloned.1.call-start
  8.0 0.7 all-gather.7.cloned.1.call-update
  8.7 0.0 reduce-scatter.3.cloned.1.call-start
  8.7 1.1 copy.21
  9.8 43.4 %all-gather.5.cloned.1.call-done = bf16[2048,256]{1,0:T(8,128)(2,1)} async-done(((bf16[256,256]{1,0:T(8,128)(2,1)}), bf16[2048,256]{1,0:T(8,128)(2,1)}) %all-gather.5.cloned.1.call-update) | async-done | bytes 1048592 | tf_op jit(solution)/shard_map/all_gather | solution.py:32
  53.2 0.0 copy-done
  53.2 0.0 copy-start.2
  53.2 2.3 fusion.6
  55.4 0.0 copy-done.2
  55.4 1.5 fusion.7
  56.9 0.0 reduce-scatter.3.cloned.1.call-update
  57.0 0.0 copy-start.1
  57.0 0.0 reduce-scatter.5.cloned.1.call-start
  57.0 37.3 %all-gather.7.cloned.1.call-done = bf16[2048,256]{1,0:T(8,128)(2,1)} async-done(((bf16[256,256]{1,0:T(8,128)(2,1)}), bf16[2048,256]{1,0:T(8,128)(2,1)}) %all-gather.7.cloned.1.call-update) | async-done | bytes 1048592 | tf_op jit(solution)/shard_map/all_gather | solution.py:33
  94.3 0.0 copy-start.3
  94.3 2.3 fusion.8
  96.6 0.0 copy-done.3
  96.6 1.5 fusion.9
  98.1 0.0 reduce-scatter.5.cloned.1.call-update
  98.1 0.0 all-gather.9.cloned.1.call-start
  98.2 60.9 %reduce-scatter.3.cloned.1.call-done = f32[32,256]{1,0:T(8,128)} async-done(((f32[256,256]{1,0:T(8,128)}), f32[32,256]{1,0:T(8,128)}) %reduce-scatter.3.cloned.1.call-update) | async-done | bytes 32784 | tf_op jit(solution)/shard_map/reduce_scatter | solution.py:40
  159.0 1.4 add_divide_fusion.1
  160.5 30.9 %all_gather.19 = f32[256,256]{1,0:T(8,128)S(1)} all-gather(f32[32,256]{1,0:T(8,128)S(1)} %get-tuple-element.31), channel_id=1, replica_groups=mesh['fs'=8,'tp'=4] {'fs'}, dimensions={0}, use_global_device_ids=true | all-gather | bytes 294912 | tf_op jit(solution)/shard_map/all_gather | solution.py:52
  191.4 0.0 copy-done.1
  191.4 1.7 multiply_reduce_fusion.1
  193.1 30.8 %reduce-scatter.5.cloned.1.call-done = f32[32,256]{1,0:T(8,128)} async-done(((f32[256,256]{1,0:T(8,128)}), f32[32,256]{1,0:T(8,128)}) %reduce-scatter.5.cloned.1.call-update) | async-done | bytes 32784 | tf_op jit(solution)/shard_map/reduce_scatter | solution.py:41
  223.9 1.4 add_divide_fusion
  225.3 30.9 %all_gather.21 = f32[256,256]{1,0:T(8,128)S(1)} all-gather(f32[32,256]{1,0:T(8,128)S(1)} %get-tuple-element.28), channel_id=1, replica_groups=mesh['fs'=8,'tp'=4] {'fs'}, dimensions={0}, use_global_device_ids=true | all-gather | bytes 294912 | tf_op jit(solution)/shard_map/all_gather | solution.py:53
  256.2 2.6 multiply_reduce_fusion
  258.8 37.9 %all-reduce = (f32[]{:T(128)}, f32[]{:T(128)}) all-reduce(f32[]{:T(128)} %get-tuple-element.34, f32[]{:T(128)} %get-tuple-element.36), channel_id=1, replica_groups=mesh['fs'=8,'tp'=4] {'fs','tp'}, use_global_device_ids=true, to_apply=%region_2.0 | all-reduce | flops 2 | bytes 16 | tf_op jit(solution)/shard_map/psum | solution.py:57
  297.4 1.8 fusion.3
  299.3 0.0 all-gather.9.cloned.1.call-update
  299.3 0.0 all-gather.11.cloned.1.call-start
  299.3 1.8 copy.22
  301.8 1.8 fusion.2
  303.6 0.0 all-gather.11.cloned.1.call-update
  303.7 1.8 copy.25
  305.4 1.8 copy.23
  307.2 1.8 copy.26
  309.0 0.8 copy.24
  309.9 29.7 %all-gather.9.cloned.1.call-done = bf16[2048,256]{0,1:T(8,128)(2,1)} async-done(((bf16[256,256]{0,1:T(8,128)(2,1)}), bf16[2048,256]{0,1:T(8,128)(2,1)}) %all-gather.9.cloned.1.call-update) | async-done | bytes 1048592 | tf_op jit(solution)/shard_map/all_gather | solution.py:66
  339.6 2.3 copy.27
  341.8 38.1 %all-gather.11.cloned.1.call-done = bf16[2048,256]{0,1:T(8,128)(2,1)} async-done(((bf16[256,256]{0,1:T(8,128)(2,1)}), bf16[2048,256]{0,1:T(8,128)(2,1)}) %all-gather.11.cloned.1.call-update) | async-done | bytes 1048592 | tf_op jit(solution)/shard_map/all_gather | solution.py:67
  379.9 2.3 copy.28
Async XLA Ops:
  7.2 46.0 %copy-start = (bf16[768,2048]{1,0:T(8,128)(2,1)S(1)}, bf16[768,2048]{1,0:T(8,128)(2,1)}, u32[]{:S(2)}) copy-start(bf16[768,2048]{1,0:T(8,128)(2,1)} %param.11) | copy-start | bytes 9437188
  7.2 46.0 %all-gather.5.cloned.1.call-start = ((), (), s32[]{:S(2)}) async-start(), calls=%async_computation.2 | async-start | bytes 1179648 | tf_op jit(solution)/shard_map/all_gather | solution.py:32
  7.9 86.4 %all-gather.7.cloned.1.call-start = ((), (), s32[]{:S(2)}) async-start(), calls=%async_computation.4 | async-start | bytes 1179648 | tf_op jit(solution)/shard_map/all_gather | solution.py:33
  8.7 150.4 %reduce-scatter.3.cloned.1.call-start = ((), (), s32[]{:S(2)}) async-start(), calls=%async_computation.3 | async-start | bytes 294912 | tf_op jit(solution)/shard_map/reduce_scatter | solution.py:40
  53.2 2.3 copy-start.2
  57.0 134.4 %copy-start.1 = (bf16[256,256]{1,0:T(8,128)(2,1)S(1)}, bf16[256,256]{1,0:T(8,128)(2,1)}, u32[]{:S(2)}) copy-start(bf16[256,256]{1,0:T(8,128)(2,1)} %param.14) | copy-start | bytes 393220
  57.0 166.9 %reduce-scatter.5.cloned.1.call-start = ((), (), s32[]{:S(2)}) async-start(), calls=%async_computation.5 | async-start | bytes 294912 | tf_op jit(solution)/shard_map/reduce_scatter | solution.py:41
  94.3 2.3 copy-start.3
  98.1 241.5 %all-gather.9.cloned.1.call-start = ((), (), s32[]{:S(2)}) async-start(), calls=%async_computation.6 | async-start | bytes 1179648 | tf_op jit(solution)/shard_map/all_gather | solution.py:66
  299.3 80.6 %all-gather.11.cloned.1.call-start = ((), (), s32[]{:S(2)}) async-start(), calls=%async_computation.7 | async-start | bytes 1179648 | tf_op jit(solution)/shard_map/all_gather | solution.py:67
Sparse Core Ops, SparseCore 0:
  10.1 42.9 all-gather.4
  55.3 38.9 all-gather.6
  98.2 60.7 reduce-scatter.2
  162.8 61.0 reduce-scatter.4
  299.4 40.1 all-gather.8
  341.5 38.3 all-gather.10
where the time goes:
time: 390 us; the launch traced here: 389 us
  waiting for transfers between devices  242 us (62%)
  blocking collectives  99.7 us (26%)
  between operations  15.6 us (4%)
  local copies, waits for them, and re-layouts  13.6 us (3%)
  matrix products  11.8 us (3%)
  other arithmetic  6.5 us (2%)
    reduce_scatter x1, waiting for transfers between devices, on_device(): lax.psum_scatter(term_in, 'fs', scatter_dimension=0, tiled=True)  60.9 us
    all_gather x1, waiting for transfers between devices, on_device(): lax.all_gather(factor_inproj, 'fs', axis=0, tiled=True)  43.4 us
    all_gather x1, waiting for transfers between devices, on_device(): lax.all_gather(fresh_out.astype(jnp.bfloat16), 'fs', axis=0, tiled=True)  38.1 us
    psum x1, blocking collectives, on_device(): lax.psum((jnp.sum(full_in * full_in), jnp.sum(full_out * full_out)), ('fs...  37.9 us
    all_gather x1, waiting for transfers between devices, on_device(): lax.all_gather(factor_outproj, 'fs', axis=0, tiled=True)  37.3 us
    all_gather x1, blocking collectives, on_device(): lax.all_gather(small_in, 'fs', axis=0, tiled=True)  30.9 us
    all_gather x1, blocking collectives, on_device(): lax.all_gather(small_out, 'fs', axis=0, tiled=True)  30.9 us
    reduce_scatter x1, waiting for transfers between devices, on_device(): lax.psum_scatter(term_out, 'fs', scatter_dimension=0, tiled=True)  30.8 us
  transfers between devices with their start and end apart: 6, of which 6 were waited for; matrix products, arithmetic and copies ran while one was open for 6% of the time, Pallas kernels for 0%

commit v1 on v0

--- a/solution.py
+++ b/solution.py
@@ -55,7 +55,7 @@
     full_in = jnp.dot(wide_in, pieces[0], precision=highest)
     full_out = jnp.dot(wide_out, pieces[1], precision=highest)
     square_in, square_out = lax.psum(
-        (jnp.sum(full_in * full_in), jnp.sum(full_out * full_out)), ("fs", "tp")
+        lax.psum((jnp.sum(full_in * full_in), jnp.sum(full_out * full_out)), "tp"), "fs"
     )
     entries = float(full_in.shape[0] * full_in.shape[1] * lax.axis_size("fs") * lax.axis_size("tp"))
     update_in = full_in / jnp.sqrt(square_in / entries + 1e-06)

time: 390 us -> 375 us (0.962)
  blocking collectives: 99.7 us -> 88.2 us
  waiting for transfers between devices: 242 us -> 238 us
    psum x1 -> x2, blocking collectives: 37.9 us -> 26.3 us  [the longest x1 20.1 us: on_device(): lax.psum(lax.psum((jnp.sum(full_in * full_in), jnp.sum(full_out * full_ou...]
where the time goes in v1:
time: 375 us; the launch traced here: 374 us
  waiting for transfers between devices  238 us (63%)
  blocking collectives  88.2 us (24%)
  between operations  15.6 us (4%)
  local copies, waits for them, and re-layouts  13.6 us (4%)
  matrix products  11.8 us (3%)
  other arithmetic  6.5 us (2%)
    reduce_scatter x1, waiting for transfers between devices, on_device(): lax.psum_scatter(term_in, 'fs', scatter_dimension=0, tiled=True)  60.9 us
    all_gather x1, waiting for transfers between devices, on_device(): lax.all_gather(factor_inproj, 'fs', axis=0, tiled=True)  43.4 us
    all_gather x1, waiting for transfers between devices, on_device(): lax.all_gather(fresh_out.astype(jnp.bfloat16), 'fs', axis=0, tiled=True)  38.1 us
    all_gather x1, waiting for transfers between devices, on_device(): lax.all_gather(factor_outproj, 'fs', axis=0, tiled=True)  37.3 us
    all_gather x1, blocking collectives, on_device(): lax.all_gather(small_in, 'fs', axis=0, tiled=True)  30.9 us
    all_gather x1, blocking collectives, on_device(): lax.all_gather(small_out, 'fs', axis=0, tiled=True)  30.9 us
    reduce_scatter x1, waiting for transfers between devices, on_device(): lax.psum_scatter(term_out, 'fs', scatter_dimension=0, tiled=True)  30.8 us
    all_gather x1, waiting for transfers between devices, on_device(): lax.all_gather(fresh_in.astype(jnp.bfloat16), 'fs', axis=0, tiled=True)  26.5 us
  transfers between devices with their start and end apart: 6, of which 6 were waited for; matrix products, arithmetic and copies ran while one was open for 6% of the time, Pallas kernels for 0%

profile of v1, /device:TPU:0, one launch (start us, length us, event | category | flops | bytes accessed | tf_op | source)
XLA Modules:
  0.0 374.2 jit_solution(2279226285364084912)
XLA Ops:
  7.2 0.0 copy-start
  7.2 0.0 all-gather.5.cloned.1.call-start
  7.2 0.7 all-gather.5.cloned.1.call-update
  7.9 0.0 all-gather.7.cloned.1.call-start
  8.0 0.7 all-gather.7.cloned.1.call-update
  8.7 0.0 reduce-scatter.3.cloned.1.call-start
  8.7 1.1 copy.21
  9.8 43.4 %all-gather.5.cloned.1.call-done = bf16[2048,256]{1,0:T(8,128)(2,1)} async-done(((bf16[256,256]{1,0:T(8,128)(2,1)}), bf16[2048,256]{1,0:T(8,128)(2,1)}) %all-gather.5.cloned.1.call-update) | async-done | bytes 1048592 | tf_op jit(solution)/shard_map/all_gather | solution.py:32
  53.2 0.0 copy-done
  53.2 0.0 copy-start.2
  53.2 2.3 fusion.6
  55.4 0.0 copy-done.2
  55.4 1.5 fusion.7
  56.9 0.0 reduce-scatter.3.cloned.1.call-update
  57.0 0.0 copy-start.1
  57.0 0.0 reduce-scatter.5.cloned.1.call-start
  57.0 37.3 %all-gather.7.cloned.1.call-done = bf16[2048,256]{1,0:T(8,128)(2,1)} async-done(((bf16[256,256]{1,0:T(8,128)(2,1)}), bf16[2048,256]{1,0:T(8,128)(2,1)}) %all-gather.7.cloned.1.call-update) | async-done | bytes 1048592 | tf_op jit(solution)/shard_map/all_gather | solution.py:33
  94.3 0.0 copy-start.3
  94.3 2.3 fusion.8
  96.6 0.0 copy-done.3
  96.6 1.5 fusion.9
  98.1 0.0 reduce-scatter.5.cloned.1.call-update
  98.1 0.0 all-gather.9.cloned.1.call-start
  98.2 60.9 %reduce-scatter.3.cloned.1.call-done = f32[32,256]{1,0:T(8,128)} async-done(((f32[256,256]{1,0:T(8,128)}), f32[32,256]{1,0:T(8,128)}) %reduce-scatter.3.cloned.1.call-update) | async-done | bytes 32784 | tf_op jit(solution)/shard_map/reduce_scatter | solution.py:40
  159.0 1.4 add_divide_fusion.1
  160.5 30.9 %all_gather.19 = f32[256,256]{1,0:T(8,128)S(1)} all-gather(f32[32,256]{1,0:T(8,128)S(1)} %get-tuple-element.33), channel_id=1, replica_groups=mesh['fs'=8,'tp'=4] {'fs'}, dimensions={0}, use_global_device_ids=true | all-gather | bytes 294912 | tf_op jit(solution)/shard_map/all_gather | solution.py:52
  191.4 0.0 copy-done.1
  191.4 1.7 multiply_reduce_fusion.1
  193.1 30.8 %reduce-scatter.5.cloned.1.call-done = f32[32,256]{1,0:T(8,128)} async-done(((f32[256,256]{1,0:T(8,128)}), f32[32,256]{1,0:T(8,128)}) %reduce-scatter.5.cloned.1.call-update) | async-done | bytes 32784 | tf_op jit(solution)/shard_map/reduce_scatter | solution.py:41
  223.9 1.4 add_divide_fusion
  225.3 30.9 %all_gather.21 = f32[256,256]{1,0:T(8,128)S(1)} all-gather(f32[32,256]{1,0:T(8,128)S(1)} %get-tuple-element.30), channel_id=1, replica_groups=mesh['fs'=8,'tp'=4] {'fs'}, dimensions={0}, use_global_device_ids=true | all-gather | bytes 294912 | tf_op jit(solution)/shard_map/all_gather | solution.py:53
  256.2 2.6 multiply_reduce_fusion
  258.8 6.3 %all-reduce.1 = (f32[]{:T(128)}, f32[]{:T(128)}) all-reduce(f32[]{:T(128)} %get-tuple-element.36, f32[]{:T(128)} %get-tuple-element.38), channel_id=1, replica_groups=mesh['fs'=8,'tp'=4] {'tp'}, use_global_device_ids=true, to_apply=%region_2.0 | all-reduce | flops 2 | bytes 16 | tf_op jit(solution)/shard_map/psum | solution.py:58
  265.1 20.1 %all-reduce = (f32[]{:T(128)}, f32[]{:T(128)}) all-reduce(f32[]{:T(128)} %get-tuple-element.22, f32[]{:T(128)} %get-tuple-element.23), channel_id=1, replica_groups=mesh['fs'=8,'tp'=4] {'fs'}, use_global_device_ids=true, to_apply=%region_3.0 | all-reduce | flops 2 | bytes 16 | tf_op jit(solution)/shard_map/psum | solution.py:57
  285.9 1.8 fusion.3
  287.7 0.0 all-gather.9.cloned.1.call-update
  287.7 0.0 all-gather.11.cloned.1.call-start
  287.8 1.8 copy.22
  290.3 1.8 fusion.2
  292.1 0.0 all-gather.11.cloned.1.call-update
  292.1 1.8 copy.25
  293.9 1.8 copy.23
  295.7 1.8 copy.26
  297.5 0.8 copy.24
  298.3 26.5 %all-gather.9.cloned.1.call-done = bf16[2048,256]{0,1:T(8,128)(2,1)} async-done(((bf16[256,256]{0,1:T(8,128)(2,1)}), bf16[2048,256]{0,1:T(8,128)(2,1)}) %all-gather.9.cloned.1.call-update) | async-done | bytes 1048592 | tf_op jit(solution)/shard_map/all_gather | solution.py:66
  324.8 2.3 copy.27
  327.0 38.1 %all-gather.11.cloned.1.call-done = bf16[2048,256]{0,1:T(8,128)(2,1)} async-done(((bf16[256,256]{0,1:T(8,128)(2,1)}), bf16[2048,256]{0,1:T(8,128)(2,1)}) %all-gather.11.cloned.1.call-update) | async-done | bytes 1048592 | tf_op jit(solution)/shard_map/all_gather | solution.py:67
  365.1 2.3 copy.28
Async XLA Ops:
  7.2 46.0 %copy-start = (bf16[768,2048]{1,0:T(8,128)(2,1)S(1)}, bf16[768,2048]{1,0:T(8,128)(2,1)}, u32[]{:S(2)}) copy-start(bf16[768,2048]{1,0:T(8,128)(2,1)} %param.11) | copy-start | bytes 9437188
  7.2 46.0 %all-gather.5.cloned.1.call-start = ((), (), s32[]{:S(2)}) async-start(), calls=%async_computation.2 | async-start | bytes 1179648 | tf_op jit(solution)/shard_map/all_gather | solution.py:32
  7.9 86.4 %all-gather.7.cloned.1.call-start = ((), (), s32[]{:S(2)}) async-start(), calls=%async_computation.4 | async-start | bytes 1179648 | tf_op jit(solution)/shard_map/all_gather | solution.py:33
  8.7 150.4 %reduce-scatter.3.cloned.1.call-start = ((), (), s32[]{:S(2)}) async-start(), calls=%async_computation.3 | async-start | bytes 294912 | tf_op jit(solution)/shard_map/reduce_scatter | solution.py:40
  53.2 2.3 copy-start.2
  57.0 134.4 %copy-start.1 = (bf16[256,256]{1,0:T(8,128)(2,1)S(1)}, bf16[256,256]{1,0:T(8,128)(2,1)}, u32[]{:S(2)}) copy-start(bf16[256,256]{1,0:T(8,128)(2,1)} %param.14) | copy-start | bytes 393220
  57.0 166.9 %reduce-scatter.5.cloned.1.call-start = ((), (), s32[]{:S(2)}) async-start(), calls=%async_computation.5 | async-start | bytes 294912 | tf_op jit(solution)/shard_map/reduce_scatter | solution.py:41
  94.3 2.3 copy-start.3
  98.1 226.7 %all-gather.9.cloned.1.call-start = ((), (), s32[]{:S(2)}) async-start(), calls=%async_computation.6 | async-start | bytes 1179648 | tf_op jit(solution)/shard_map/all_gather | solution.py:66
  287.7 77.4 %all-gather.11.cloned.1.call-start = ((), (), s32[]{:S(2)}) async-start(), calls=%async_computation.7 | async-start | bytes 1179648 | tf_op jit(solution)/shard_map/all_gather | solution.py:67
Sparse Core Ops, SparseCore 0:
  10.1 42.9 all-gather.4
  55.3 38.9 all-gather.6
  98.2 60.7 reduce-scatter.2
  162.8 61.0 reduce-scatter.4
  287.9 36.8 all-gather.8
  326.7 38.3 all-gather.10
